TPU v7x, 512 devices: a whole 4x8x8 slice. The times are simulated.
512 devices in a mesh: sp: 64 (over z, y), tp: 4 (over x), dp: 2 (over core).
Axes of the slice: x: 4, y: 8, z: 8, core: 2. Of those that a mesh axis runs over, the one named last changes fastest.
Arguments:
- latent: bfloat16 [2, 16384, 2048], P('dp', ('sp', 'tp')), may hold values from -6 to 6
- condition: bfloat16 [2, 2048], P('dp', ('sp', 'tp')), may hold values from -6 to 6
- context: bfloat16 [2, 512, 2048], P('dp', 'sp'), may hold values from -6 to 6
- context_vector: bfloat16 [2048], P(('sp', 'tp')), may hold values from -6 to 6
- modulator: bfloat16 [2048, 6144], P(('sp', 'tp')), may hold values from -0.3125 to 0.3125
- norm_gain: float32 [2048], replicated, may hold values from 0.1 to 1.9
- query_weight: bfloat16 [2048, 512], P(None, 'tp'), may hold values from -4 to 4
- key_weight: bfloat16 [2048, 512], P(None, 'tp'), may hold values from -0.125 to 0.125
- value_weight: bfloat16 [2048, 512], P(None, 'tp'), may hold values from -0.125 to 0.125
- head_gain: float32 [128], replicated, may hold values from 0.1 to 1.9
- lambdas: float32 [4], P('tp'), may hold values from 0.3 to 0.8
- context_bias: float32 [4, 2], P('tp'), may hold values from 1.3 to 2.7
- out_weight: bfloat16 [512, 2048], P('tp'), may hold values from -0.25 to 0.25
Outputs:
- updated: bfloat16 [2, 16384, 2048], P('dp', ('sp', 'tp'))
All inputs are finite; a program needn't handle non-finite values.
Results may differ from a plain program's by a relative error of at most 0.024.
Values may be sent and summed in bfloat16 or wider, within the bound.
A program may use at most 64 MiB of HBM per device.

v0:
```python
import jax
import jax.numpy as jnp
from jax import lax
from jax.sharding import Mesh
from jax.sharding import PartitionSpec as P

SP_TP = ("sp_0", "sp_1", "tp")
SP = ("sp_0", "sp_1")
EPSILON = 1e-06
OUT_SCALE = 0.8
KEY_BLOCK = 2048
LOW_START = -1e30


def by_axis(shard, axes):
    for axis in axes:
        shard = lax.psum(shard, axis)
    return shard


def joined_along(blocks, dim):
    lengths = list(blocks.shape[1:])
    lengths[dim] *= blocks.shape[0]
    return jnp.moveaxis(blocks, 0, dim).reshape(lengths)


def sent_to_all(shard, axis):
    copies = jnp.broadcast_to(shard, (lax.axis_size(axis), *shard.shape))
    return lax.all_to_all(copies, axis, split_axis=0, concat_axis=0, tiled=True)


def gather_directly(shard, axis, dim):
    return joined_along(sent_to_all(shard, axis), dim)


def sent_together(arrays, axis, dim, along):
    ends, at = ([], 0)
    for a in arrays[:-1]:
        at += a.shape[along]
        ends.append(at)
    both = jnp.concatenate(arrays, axis=along)
    return tuple(jnp.split(lax.all_gather(both, axis, axis=dim, tiled=True), ends, axis=along))


def split_up(shard, dim, devices):
    lengths = shard.shape
    blocks = shard.reshape(*lengths[:dim], devices, lengths[dim] // devices, *lengths[dim + 1 :])
    return jnp.moveaxis(blocks, dim, 0)


def summed_on_arrival(shard, axis, dim):
    blocks = split_up(shard, dim, lax.axis_size(axis))
    arrived = lax.all_to_all(blocks, axis, split_axis=0, concat_axis=0, tiled=True)
    return arrived.astype(jnp.float32).sum(axis=0)


def modulate(inputs, gain_vector, shift_vector, scale_vector):
    as_float = inputs.astype(jnp.float32)
    normed = as_float * lax.rsqrt(jnp.mean(as_float * as_float, axis=-1, keepdims=True) + EPSILON)
    return (normed * gain_vector * (1.0 + scale_vector) + shift_vector).astype(jnp.bfloat16)


def fold_block(running, queries, keys_in, values_in, key_flags, bias_table, score_scale):
    run_max, run_total, summed = running
    scores = (
        jnp.einsum("qhmd,khmd->hmqk", queries, keys_in, preferred_element_type=jnp.float32)
        * score_scale
    )
    if key_flags is not None:
        scores = scores + bias_table[:, :, None, None] * key_flags
    new_max = jnp.maximum(run_max, jnp.max(scores, axis=-1))
    shrink = jnp.exp(run_max - new_max)
    weights = jnp.exp(scores - new_max[..., None])
    run_total = run_total * shrink + jnp.sum(weights, axis=-1)
    summed = summed * shrink[..., None] + jnp.einsum(
        "hmqk,khe->hmqe",
        weights.astype(jnp.bfloat16),
        values_in,
        preferred_element_type=jnp.float32,
    )
    return (new_max, run_total, summed)


def fold_keys(running, queries, keys_in, values_in, key_flags, bias_table, score_scale):
    full_blocks = keys_in.shape[0] // KEY_BLOCK
    if full_blocks > 1:
        edge = full_blocks * KEY_BLOCK
        stacked = (
            keys_in.reshape((full_blocks, KEY_BLOCK) + keys_in.shape[1:]),
            values_in.reshape((full_blocks, KEY_BLOCK) + values_in.shape[1:]),
        )

        def fold_step(current, block_data):
            flag_part = None
            return (
                fold_block(
                    current,
                    queries,
                    block_data[0],
                    block_data[1],
                    flag_part,
                    bias_table,
                    score_scale,
                ),
                None,
            )

        running, ignored = lax.scan(fold_step, running, stacked)
        keys_in = keys_in[edge:]
        values_in = values_in[edge:]
        key_flags = None
    if keys_in.shape[0] > 0:
        running = fold_block(
            running, queries, keys_in, values_in, key_flags, bias_table, score_scale
        )
    return running


def body(
    latent,
    condition,
    context,
    context_vector,
    modulator,
    norm_gain,
    query_weight,
    key_weight,
    value_weight,
    head_gain,
    lambdas,
    context_bias,
    out_weight,
):
    model_width = latent.shape[2]
    local_heads = lambdas.shape[0]
    query_width = query_weight.shape[1]
    head_size = query_width // (2 * local_heads)
    value_size = value_weight.shape[1] // local_heads
    score_scale = head_size ** (-0.5)
    activated = jax.nn.silu(
        jnp.concatenate([condition, context_vector[None, :]], axis=0).astype(jnp.float32)
    )
    partial_terms = jnp.dot(
        activated.astype(jnp.bfloat16), modulator, preferred_element_type=jnp.float32
    )
    modulations = by_axis(partial_terms, SP_TP)
    hidden = modulate(
        latent[0],
        norm_gain,
        modulations[0, :model_width],
        modulations[0, model_width : 2 * model_width],
    )
    ctx_hidden = modulate(
        context[0],
        norm_gain,
        modulations[1, :model_width],
        modulations[1, model_width : 2 * model_width],
    )
    gate_vector = modulations[0, 2 * model_width :]
    incoming = gather_directly(hidden, "tp", 0)
    projected = jnp.concatenate(
        [
            jnp.dot(incoming, query_weight, preferred_element_type=jnp.float32),
            jnp.dot(incoming, key_weight, preferred_element_type=jnp.float32),
            jnp.dot(incoming, value_weight, preferred_element_type=jnp.float32),
        ],
        axis=1,
    ).astype(jnp.bfloat16)
    query_rows = projected.shape[0]
    queries = projected[:, :query_width].reshape(query_rows, local_heads, 2, head_size)
    own_keys = projected[:, query_width : 2 * query_width]
    own_values = projected[:, 2 * query_width :]
    ctx_keys = jnp.dot(ctx_hidden, key_weight, preferred_element_type=jnp.float32).astype(
        jnp.bfloat16
    )
    ctx_values = jnp.dot(ctx_hidden, value_weight, preferred_element_type=jnp.float32).astype(
        jnp.bfloat16
    )
    ctx_keys, ctx_values = sent_together((ctx_keys, ctx_values), SP, 0, 1)
    start_carry = (
        jnp.full((local_heads, 2, query_rows), LOW_START, jnp.float32),
        jnp.zeros((local_heads, 2, query_rows), jnp.float32),
        jnp.zeros((local_heads, 2, query_rows, value_size), jnp.float32),
    )
    pieces = (own_keys, own_values)
    initial = fold_keys(
        start_carry,
        queries,
        ctx_keys.reshape(-1, local_heads, 2, head_size),
        ctx_values.reshape(-1, local_heads, value_size),
        jnp.ones((ctx_keys.shape[0],), jnp.float32),
        context_bias,
        score_scale,
    )
    incoming = sent_together((pieces[0], pieces[1]), SP, 0, 1)
    run_max, run_total, summed = fold_keys(
        initial,
        queries,
        incoming[0].reshape(-1, local_heads, 2, head_size),
        incoming[1].reshape(-1, local_heads, value_size),
        None,
        context_bias,
        score_scale,
    )
    mixed = (
        summed[:, 0] / run_total[:, 0, :, None]
        - lambdas[:, None, None] * summed[:, 1] / run_total[:, 1, :, None]
    )
    normed = (
        mixed
        * lax.rsqrt(jnp.mean(mixed * mixed, axis=-1, keepdims=True) + EPSILON)
        * head_gain
        * OUT_SCALE
    )
    attended = (
        jnp.transpose(normed, (1, 0, 2))
        .reshape(query_rows, local_heads * value_size)
        .astype(jnp.bfloat16)
    )
    branch = summed_on_arrival(
        jnp.dot(attended, out_weight, preferred_element_type=jnp.float32).astype(jnp.bfloat16),
        "tp",
        0,
    )
    result = (latent[0].astype(jnp.float32) + gate_vector * branch).astype(jnp.bfloat16)
    return result[None]


def solution(mesh):
    torus = Mesh(
        mesh.devices.reshape(8, 8, mesh.shape["tp"], mesh.shape["dp"]), ("sp_0", "sp_1", "tp", "dp")
    )
    return jax.shard_map(
        body,
        mesh=torus,
        in_specs=(
            P("dp", SP_TP, None),
            P("dp", SP_TP),
            P("dp", SP, None),
            P(SP_TP),
            P(SP_TP, None),
            P(),
            P(None, "tp"),
            P(None, "tp"),
            P(None, "tp"),
            P(),
            P("tp"),
            P("tp", None),
            P("tp", None),
        ),
        out_specs=P("dp", SP_TP, None),
        check_vma=False,
    )
```

profile of v0, /device:TPU:8, one launch (start us, length us, event | category | flops | bytes accessed | tf_op | source)
XLA Modules:
  0.0 289.6 jit_solution(1332967432429290090)
XLA Ops:
  7.8 36.4 %psum.21 = f32[2,6144]{1,0:T(2,128)S(1)} all-reduce(f32[2,6144]{1,0:T(2,128)S(1)} %fusion.60), channel_id=1, replica_groups=mesh['sp_0'=8,'sp_1'=8,'tp'=4,'dp'=2] {'sp_0'}, use_global_device_ids=true, to_apply=%region_0.1 | all-reduce | flops 12288 | bytes 98304 | tf_op jit(solution)/shard_map/psum | solution.py:17
  44.2 28.8 %psum.22 = f32[2,6144]{1,0:T(2,128)S(1)} all-reduce(f32[2,6144]{1,0:T(2,128)S(1)} %psum.21), channel_id=1, replica_groups=mesh['sp_0'=8,'sp_1'=8,'tp'=4,'dp'=2] {'sp_1'}, use_global_device_ids=true, to_apply=%region_1.2 | all-reduce | flops 12288 | bytes 98304 | tf_op jit(solution)/shard_map/psum | solution.py:17
  72.9 17.9 %psum.23 = f32[2,6144]{1,0:T(2,128)S(1)} all-reduce(f32[2,6144]{1,0:T(2,128)S(1)} %psum.22), channel_id=1, replica_groups=mesh['sp_0'=8,'sp_1'=8,'tp'=4,'dp'=2] {'tp'}, use_global_device_ids=true, to_apply=%region_2.3 | all-reduce | flops 12288 | bytes 98304 | tf_op jit(solution)/shard_map/psum | solution.py:17
  93.3 13.5 %all_to_all.10 = bf16[4,64,2048]{2,1,0:T(8,128)(2,1)S(1)} all-to-all(bf16[4,64,2048]{2,1,0:T(8,128)(2,1)S(1)} %broadcast_in_dim.13), channel_id=1, replica_groups=mesh['sp_0'=8,'sp_1'=8,'tp'=4,'dp'=2] {'tp'}, dimensions={0} | all-to-all | bytes 2097152 | tf_op jit(solution)/shard_map/all_to_all | solution.py:29
  109.1 49.1 %all_gather.6 = bf16[512,256]{1,0:T(8,128)(2,1)S(1)} all-gather(bf16[8,256]{1,0:T(8,128)(2,1)S(1)} %pad_maximum_fusion.1), channel_id=1, replica_groups=mesh['sp_0'=8,'sp_1'=8,'tp'=4,'dp'=2] {'sp_0','sp_1'}, dimensions={0}, use_global_device_ids=true | all-gather | bytes 266240 | tf_op jit(solution)/shard_map/all_gather | solution.py:42
  160.7 50.3 %all-gather.2.cloned.1.call-done = bf16[16384,256]{0,1:T(8,128)(2,1)} async-done(((bf16[256,256]{0,1:T(8,128)(2,1)}), bf16[16384,256]{0,1:T(8,128)(2,1)}) %all-gather.2.cloned.1.call-update) | async-done | bytes 8388624 | tf_op jit(solution)/shard_map/all_gather | solution.py:42
  211.0 5.0 %fusion.72 = (bf16[16384,128]{0,1:T(8,128)(2,1)}, bf16[16384,128]{0,1:T(8,128)(2,1)S(1)}) fusion(bf16[16384,256]{0,1:T(8,128)(2,1)} %all-gather.2.cloned.1.call-done), kind=kLoop, calls=%fused_computation.100 | loop fusion | bytes 16777216 | tf_op jit(solution)/shard_map/split | solution.py:42
  216.0 3.2 %copy.24 = bf16[16,8,8,2048]{3,2,1,0:T(8,128)(2,1)S(1)} copy(bf16[16,8,8,2048]{3,1,2,0:T(8,128)(2,1)S(1)} %bitcast.170) | data formatting | bytes 8388608
  219.2 4.2 %copy.20 = bf16[8,2048,1,2,64]{1,4,3,2,0:T(8,128)(2,1)} copy(bf16[8,2048,1,2,64]{1,0,4,3,2:T(8,128)(2,1)S(1)} %bitcast.166) | data formatting | bytes 8388608 | tf_op jit(solution)/shard_map/while | solution.py:108
  223.4 6.4 %copy.23 = bf16[16384,128]{1,0:T(8,128)(2,1)} copy(bf16[16384,128]{0,1:T(8,128)(2,1)} %get-tuple-element.77) | data formatting | bytes 8388608 | tf_op jit(solution)/shard_map/while | solution.py:108
  229.8 36.3 %while.14 = (s32[]{:T(128)}, f32[1,2,256]{2,1,0:T(2,128)S(1)}, f32[1,2,256]{2,1,0:T(2,128)S(1)}, f32[1,2,256,128]{3,2,1,0:T(8,128)S(1)}, bf16[8,2048,1,2,64]{1,4...) while((s32[]{:T(128)}, f32[1,2,256]{2,1,0:T(2,128)S(1)}, ...), condition=%wide.region_10.11_spmd, body=%wide.region_7.10_spmd.sunk | while | flops 411174400 | bytes 14255189 | solution.py:108
  231.6 2.0 fusion.97
  236.2 2.0 fusion.97
  240.7 2.0 fusion.97
  243.4 1.8 bitcast_reduce_fusion.2
  245.2 2.0 fusion.97
  247.9 1.8 bitcast_reduce_fusion.2
  249.8 2.0 fusion.97
  254.3 2.0 fusion.97
  257.0 1.8 bitcast_reduce_fusion.2
  258.9 2.0 fusion.97
  261.6 1.8 bitcast_reduce_fusion.2
  263.4 2.0 fusion.97
  266.9 14.9 %all_to_all.11 = bf16[4,64,2048]{2,1,0:T(8,128)(2,1)S(1)} all-to-all(bf16[4,64,2048]{2,1,0:T(8,128)(2,1)S(1)} %bitcast.172), channel_id=1, replica_groups=mesh['sp_0'=8,'sp_1'=8,'tp'=4,'dp'=2] {'tp'}, dimensions={0} | all-to-all | bytes 2097152 | tf_op jit(solution)/shard_map/all_to_all | solution.py:53
  (84 shorter events, 22.4 us)
Async XLA Ops:
  6.5 259.8 %copy-start = (bf16[128,2048]{1,0:T(8,128)(2,1)S(1)}, bf16[128,2048]{1,0:T(8,128)(2,1)}, u32[]{:S(2)}) copy-start(bf16[128,2048]{1,0:T(8,128)(2,1)} %param.27) | copy-start | bytes 1572868
  6.5 100.3 %copy-start.2 = (bf16[2048,128]{1,0:T(8,128)(2,1)S(1)}, bf16[2048,128]{1,0:T(8,128)(2,1)}, u32[]{:S(2)}) copy-start(bf16[2048,128]{1,0:T(8,128)(2,1)} %param.23) | copy-start | bytes 1572868
  6.5 100.8 %copy-start.3 = (bf16[2048,128]{1,0:T(8,128)(2,1)S(1)}, bf16[2048,128]{1,0:T(8,128)(2,1)}, u32[]{:S(2)}) copy-start(bf16[2048,128]{1,0:T(8,128)(2,1)} %param.22) | copy-start | bytes 1572868
  6.5 204.4 %all-gather.2.cloned.1.call-start = ((), (), s32[]{:S(2)}) async-start(), calls=%async_computation.2 | async-start | bytes 8519680 | tf_op jit(solution)/shard_map/all_gather | solution.py:42
  6.5 102.0 %copy-start.5 = (bf16[1,8,2048]{2,1,0:T(8,128)(2,1)S(1)}, bf16[1,8,2048]{2,1,0:T(8,128)(2,1)}, u32[]{:S(2)}) copy-start(bf16[1,8,2048]{2,1,0:T(8,128)(2,1)} %param.17) | copy-start | bytes 98308
  7.8 100.9 %copy-start.6 = (f32[2048]{0:T(1024)S(1)}, f32[2048]{0:T(1024)}, u32[]{:S(2)}) copy-start(f32[2048]{0:T(1024)} %param.20) | copy-start | bytes 24580
  93.3 65.7 %copy-start.4 = (bf16[2048,128]{1,0:T(8,128)(2,1)S(1)}, bf16[2048,128]{1,0:T(8,128)(2,1)}, u32[]{:S(2)}) copy-start(bf16[2048,128]{1,0:T(8,128)(2,1)} %param.21) | copy-start | bytes 1572868
  93.3 66.2 %copy-start.7 = (f32[1,2]{1,0:T(1,128)S(1)}, f32[1,2]{1,0:T(1,128)}, u32[]{:S(2)}) copy-start(f32[1,2]{1,0:T(1,128)} %param.26) | copy-start | bytes 28
  229.8 36.6 %copy-start.8 = (f32[128]{0:T(128)S(1)}, f32[128]{0:T(128)}, u32[]{:S(2)}) copy-start(f32[128]{0:T(128)} %param.24) | copy-start | bytes 1540
  266.1 15.9 %copy-start.1 = (bf16[1,64,2048]{2,1,0:T(8,128)(2,1)S(1)}, bf16[1,64,2048]{2,1,0:T(8,128)(2,1)}, u32[]{:S(2)}) copy-start(bf16[1,64,2048]{2,1,0:T(8,128)(2,1)} %param.15) | copy-start | bytes 786436
Sparse Core Ops, SparseCore 0:
  108.6 102.3 all-gather.1
where the time goes:
time: 291 us; the launch traced here: 290 us
  blocking collectives  161 us (55%)
  waiting for transfers between devices  50.3 us (17%)
  matrix products  34.6 us (12%)
  local copies, waits for them, and re-layouts  19.1 us (7%)
  between operations  14.3 us (5%)
  other arithmetic  10.4 us (4%)
    psum x3, blocking collectives, by_axis(): shard = lax.psum(shard, axis)  83.1 us
    all_gather x1, waiting for transfers between devices, sent_together(): lax.all_gather(both, axis, axis=dim, tiled=True)  50.3 us
    all_gather x1, blocking collectives, sent_together(): lax.all_gather(both, axis, axis=dim, tiled=True)  49.1 us
    dot_general x9, matrix products, fold_block(): jnp.einsum('hmqk,khe->hmqe', weights.astype(jnp.bfloat16), values_in, pre...  16 us
    dot_general x9, matrix products, fold_block(): jnp.einsum('qhmd,khmd->hmqk', queries, keys_in, preferred_element_type=jn...  14.9 us
    all_to_all x1, blocking collectives, summed_on_arrival(): lax.all_to_all(blocks, axis, split_axis=0, concat_axis=0, tiled=True)  14.9 us
    all_to_all x1, blocking collectives, sent_to_all(): return lax.all_to_all(copies, axis, split_axis=0, concat_axis=0, tiled=True)  13.5 us
    while x2, local copies, waits for them, and re-layouts, fold_keys(): running, ignored = lax.scan(fold_step, running, stacked)  10.6 us
  transfers between devices with their start and end apart: 1, of which 1 were waited for; matrix products, arithmetic and copies ran while one was open for 1% of the time, Pallas kernels for 0%

commit v1 on v0

--- a/solution.py
+++ b/solution.py
@@ -14,7 +14,7 @@
 
 def by_axis(shard, axes):
     for axis in axes:
-        shard = lax.psum(shard, axis)
+        shard = jnp.sum(lax.all_gather(shard, axis), axis=0)
     return shard
 
 

time: 291 us -> 281 us (0.966)
  blocking collectives: 161 us -> 149 us
    psum x3 -> x0, blocking collectives: 83.1 us -> none  [by_axis(): shard = lax.psum(shard, axis)]
    all_gather x0 -> x3, blocking collectives: none -> 70.4 us  [by_axis(): shard = jnp.sum(lax.all_gather(shard, axis), axis=0)]
where the time goes in v1:
time: 281 us; the launch traced here: 280 us
  blocking collectives  149 us (53%)
  waiting for transfers between devices  51.6 us (18%)
  matrix products  34.6 us (12%)
  local copies, waits for them, and re-layouts  19.1 us (7%)
  between operations  14.3 us (5%)
  other arithmetic  10.7 us (4%)
    all_gather x3, blocking collectives, by_axis(): shard = jnp.sum(lax.all_gather(shard, axis), axis=0)  70.4 us
    all_gather x1, waiting for transfers between devices, sent_together(): lax.all_gather(both, axis, axis=dim, tiled=True)  51.6 us
    all_gather x1, blocking collectives, sent_together(): lax.all_gather(both, axis, axis=dim, tiled=True)  49.2 us
    dot_general x9, matrix products, fold_block(): jnp.einsum('hmqk,khe->hmqe', weights.astype(jnp.bfloat16), values_in, pre...  16 us
    dot_general x9, matrix products, fold_block(): jnp.einsum('qhmd,khmd->hmqk', queries, keys_in, preferred_element_type=jn...  14.9 us
    all_to_all x1, blocking collectives, summed_on_arrival(): lax.all_to_all(blocks, axis, split_axis=0, concat_axis=0, tiled=True)  14.9 us
    all_to_all x1, blocking collectives, sent_to_all(): return lax.all_to_all(copies, axis, split_axis=0, concat_axis=0, tiled=True)  14.4 us
    while x2, local copies, waits for them, and re-layouts, fold_keys(): running, ignored = lax.scan(fold_step, running, stacked)  10.6 us
  transfers between devices with their start and end apart: 1, of which 1 were waited for; matrix products, arithmetic and copies ran while one was open for 1% of the time, Pallas kernels for 0%

profile of v1, /device:TPU:8, one launch (start us, length us, event | category | flops | bytes accessed | tf_op | source)
XLA Modules:
  0.0 279.7 jit_solution(8007520951843445950)
XLA Ops:
  7.8 31.4 %all-gather.3 = f32[8,2,6144]{2,1,0:T(2,128)S(1)} all-gather(f32[1,2,6144]{2,1,0:T(2,128)S(1)} %convolution_bitcast_fusion), channel_id=2, replica_groups=mesh['sp_0'=8,'sp_1'=8,'tp'=4,'dp'=2] {'sp_0'}, dimensions={0}, use_global_device_ids=true | all-gather | bytes 442368 | tf_op jit(solution)/shard_map/all_gather | solution.py:17
  39.3 25.8 %all-gather.4 = f32[8,2,6144]{2,1,0:T(2,128)S(1)} all-gather(f32[1,2,6144]{2,1,0:T(2,128)S(1)} %bitcast.182), channel_id=3, replica_groups=mesh['sp_0'=8,'sp_1'=8,'tp'=4,'dp'=2] {'sp_1'}, dimensions={0}, use_global_device_ids=true | all-gather | bytes 442368 | tf_op jit(solution)/shard_map/all_gather | solution.py:17
  65.2 13.2 %all-gather.5 = f32[4,2,6144]{2,1,0:T(2,128)S(1)} all-gather(f32[1,2,6144]{2,1,0:T(2,128)S(1)} %bitcast.183), channel_id=4, replica_groups=mesh['sp_0'=8,'sp_1'=8,'tp'=4,'dp'=2] {'tp'}, dimensions={0}, use_global_device_ids=true | all-gather | bytes 245760 | tf_op jit(solution)/shard_map/all_gather | solution.py:17
  81.0 14.4 %all_to_all.10 = bf16[4,64,2048]{2,1,0:T(8,128)(2,1)S(1)} all-to-all(bf16[4,64,2048]{2,1,0:T(8,128)(2,1)S(1)} %broadcast_in_dim.13), channel_id=1, replica_groups=mesh['sp_0'=8,'sp_1'=8,'tp'=4,'dp'=2] {'tp'}, dimensions={0} | all-to-all | bytes 2097152 | tf_op jit(solution)/shard_map/all_to_all | solution.py:29
  97.7 49.2 %all_gather.30 = bf16[512,256]{1,0:T(8,128)(2,1)S(1)} all-gather(bf16[8,256]{1,0:T(8,128)(2,1)S(1)} %pad_maximum_fusion.1), channel_id=1, replica_groups=mesh['sp_0'=8,'sp_1'=8,'tp'=4,'dp'=2] {'sp_0','sp_1'}, dimensions={0}, use_global_device_ids=true | all-gather | bytes 266240 | tf_op jit(solution)/shard_map/all_gather | solution.py:42
  149.4 51.6 %all-gather.8.cloned.1.call-done = bf16[16384,256]{0,1:T(8,128)(2,1)} async-done(((bf16[256,256]{0,1:T(8,128)(2,1)}), bf16[16384,256]{0,1:T(8,128)(2,1)}) %all-gather.8.cloned.1.call-update) | async-done | bytes 8388624 | tf_op jit(solution)/shard_map/all_gather | solution.py:42
  201.0 5.0 %fusion.71 = (bf16[16384,128]{0,1:T(8,128)(2,1)}, bf16[16384,128]{0,1:T(8,128)(2,1)S(1)}) fusion(bf16[16384,256]{0,1:T(8,128)(2,1)} %all-gather.8.cloned.1.call-done), kind=kLoop, calls=%fused_computation.100 | loop fusion | bytes 16777216 | tf_op jit(solution)/shard_map/split | solution.py:42
  206.1 3.2 %copy.28 = bf16[16,8,8,2048]{3,2,1,0:T(8,128)(2,1)S(1)} copy(bf16[16,8,8,2048]{3,1,2,0:T(8,128)(2,1)S(1)} %bitcast.174) | data formatting | bytes 8388608
  209.3 4.2 %copy.24 = bf16[8,2048,1,2,64]{1,4,3,2,0:T(8,128)(2,1)} copy(bf16[8,2048,1,2,64]{1,0,4,3,2:T(8,128)(2,1)S(1)} %bitcast.170) | data formatting | bytes 8388608 | tf_op jit(solution)/shard_map/while | solution.py:108
  213.5 6.4 %copy.27 = bf16[16384,128]{1,0:T(8,128)(2,1)} copy(bf16[16384,128]{0,1:T(8,128)(2,1)} %get-tuple-element.84) | data formatting | bytes 8388608 | tf_op jit(solution)/shard_map/while | solution.py:108
  219.9 36.3 %while.14 = (s32[]{:T(128)}, f32[1,2,256]{2,1,0:T(2,128)S(1)}, f32[1,2,256]{2,1,0:T(2,128)S(1)}, f32[1,2,256,128]{3,2,1,0:T(8,128)S(1)}, bf16[8,2048,1,2,64]{1,4...) while((s32[]{:T(128)}, f32[1,2,256]{2,1,0:T(2,128)S(1)}, ...), condition=%wide.region_10.11_spmd, body=%wide.region_7.10_spmd.sunk | while | flops 411174400 | bytes 14255189 | solution.py:108
  221.7 2.0 fusion.96
  226.2 2.0 fusion.96
  230.8 2.0 fusion.96
  233.5 1.8 bitcast_reduce_fusion.2
  235.3 2.0 fusion.96
  238.0 1.8 bitcast_reduce_fusion.2
  239.8 2.0 fusion.96
  244.4 2.0 fusion.96
  247.1 1.8 bitcast_reduce_fusion.2
  248.9 2.0 fusion.96
  251.6 1.8 bitcast_reduce_fusion.2
  253.5 2.0 fusion.96
  257.0 14.9 %all_to_all.11 = bf16[4,64,2048]{2,1,0:T(8,128)(2,1)S(1)} all-to-all(bf16[4,64,2048]{2,1,0:T(8,128)(2,1)S(1)} %bitcast.176), channel_id=1, replica_groups=mesh['sp_0'=8,'sp_1'=8,'tp'=4,'dp'=2] {'tp'}, dimensions={0} | all-to-all | bytes 2097152 | tf_op jit(solution)/shard_map/all_to_all | solution.py:53
  (87 shorter events, 22.8 us)
Async XLA Ops:
  6.5 249.9 %copy-start = (bf16[128,2048]{1,0:T(8,128)(2,1)S(1)}, bf16[128,2048]{1,0:T(8,128)(2,1)}, u32[]{:S(2)}) copy-start(bf16[128,2048]{1,0:T(8,128)(2,1)} %param.27) | copy-start | bytes 1572868
  6.5 88.9 %copy-start.2 = (bf16[2048,128]{1,0:T(8,128)(2,1)S(1)}, bf16[2048,128]{1,0:T(8,128)(2,1)}, u32[]{:S(2)}) copy-start(bf16[2048,128]{1,0:T(8,128)(2,1)} %param.23) | copy-start | bytes 1572868
  6.5 89.4 %copy-start.3 = (bf16[2048,128]{1,0:T(8,128)(2,1)S(1)}, bf16[2048,128]{1,0:T(8,128)(2,1)}, u32[]{:S(2)}) copy-start(bf16[2048,128]{1,0:T(8,128)(2,1)} %param.22) | copy-start | bytes 1572868
  6.5 194.5 %all-gather.8.cloned.1.call-start = ((), (), s32[]{:S(2)}) async-start(), calls=%async_computation.2 | async-start | bytes 8519680 | tf_op jit(solution)/shard_map/all_gather | solution.py:42
  65.2 31.9 %copy-start.5 = (bf16[1,8,2048]{2,1,0:T(8,128)(2,1)S(1)}, bf16[1,8,2048]{2,1,0:T(8,128)(2,1)}, u32[]{:S(2)}) copy-start(bf16[1,8,2048]{2,1,0:T(8,128)(2,1)} %param.17) | copy-start | bytes 98308
  78.5 18.8 %copy-start.6 = (f32[2048]{0:T(1024)S(1)}, f32[2048]{0:T(1024)}, u32[]{:S(2)}) copy-start(f32[2048]{0:T(1024)} %param.20) | copy-start | bytes 24580
  81.0 66.8 %copy-start.4 = (bf16[2048,128]{1,0:T(8,128)(2,1)S(1)}, bf16[2048,128]{1,0:T(8,128)(2,1)}, u32[]{:S(2)}) copy-start(bf16[2048,128]{1,0:T(8,128)(2,1)} %param.21) | copy-start | bytes 1572868
  81.0 67.3 %copy-start.7 = (f32[1,2]{1,0:T(1,128)S(1)}, f32[1,2]{1,0:T(1,128)}, u32[]{:S(2)}) copy-start(f32[1,2]{1,0:T(1,128)} %param.26) | copy-start | bytes 28
  219.9 36.6 %copy-start.8 = (f32[128]{0:T(128)S(1)}, f32[128]{0:T(128)}, u32[]{:S(2)}) copy-start(f32[128]{0:T(128)} %param.24) | copy-start | bytes 1540
  256.2 15.9 %copy-start.1 = (bf16[1,64,2048]{2,1,0:T(8,128)(2,1)S(1)}, bf16[1,64,2048]{2,1,0:T(8,128)(2,1)}, u32[]{:S(2)}) copy-start(bf16[1,64,2048]{2,1,0:T(8,128)(2,1)} %param.15) | copy-start | bytes 786436
Sparse Core Ops, SparseCore 0:
  97.2 103.7 all-gather.7
